TPU v7x, 32 devices: a whole 2x2x4 slice. The times are simulated.
32 devices in a mesh: ep: 16 (over z, y, x), tp: 2 (over core).
Axes of the slice: x: 2, y: 2, z: 4, core: 2. Of those that a mesh axis runs over, the one named last changes fastest.
Arguments:
- tokens: bfloat16 [256, 2048], P('ep'), may hold values from -6 to 6
- recurrent_state: float32 [256, 4, 128, 256], P('ep', 'tp'), may hold values from -6 to 6
- query_weight: bfloat16 [2048, 512], P(None, 'tp'), may hold values from -0.125 to 0.125
- key_weight: bfloat16 [2048, 512], P(None, 'tp'), may hold values from -0.125 to 0.125
- decay_weight: bfloat16 [2048, 512], P(None, 'tp'), may hold values from -0.5 to 0.5
- value_weight: bfloat16 [2048, 1024], P(None, 'tp'), may hold values from -0.125 to 0.125
- gate_weight: bfloat16 [2048, 1024], P(None, 'tp'), may hold values from -0.125 to 0.125
- head_gain: float32 [256], replicated, may hold values from 0.1 to 1.9
- output_weight: bfloat16 [1024, 2048], P('tp'), may hold values from -0.375 to 0.375
- norm_gain: float32 [2, 2048], replicated, may hold values from 0.1 to 1.9
- norm_bias: float32 [2, 2048], replicated, may hold values from -1.8 to 1.8
- group_router: bfloat16 [2048, 4], replicated, may hold values from -0.125 to 0.125
- router_weight: bfloat16 [2048, 32], replicated, may hold values from -0.125 to 0.125
- routes: int32 [256, 2], P('ep'), may hold values from 0 to 31, as said below
- expert_gate: bfloat16 [32, 2048, 256], P(('ep', 'tp')), may hold values from -0.125 to 0.125
- expert_up: bfloat16 [32, 2048, 256], P(('ep', 'tp')), may hold values from -0.125 to 0.125
- expert_down: bfloat16 [32, 256, 2048], P(('ep', 'tp')), may hold values from -1.5 to 1.5
Outputs:
- new_tokens: bfloat16 [256, 2048], P('ep', 'tp')
- new_state: float32 [256, 4, 128, 256], P('ep', 'tp')
Inputs may be any that keep to these rules, and one draw needn't show every extreme that they name: `routes`: each row names two different experts of one group (group g holds the experts g * 8 to g * 8 + 7). In the rows of one device each group is named by the same number of rows and no expert by more than 2 rows; some expert is named by exactly 2 rows of every device.
All inputs are finite; a program needn't handle non-finite values.
Results may differ from a plain program's by a relative error of at most 0.01.
Values may be sent and summed in bfloat16 or wider, within the bound.
A program may use at most 128 MiB of HBM per device.

v0:
```python
import functools

import jax
import jax.numpy as jnp
from jax import lax
from jax.experimental import pallas as pl
from jax.experimental.pallas import tpu as pltpu
from jax.sharding import PartitionSpec as P

MESH = pl.DeviceIdType.MESH
alpha_res = 2.0**0.5
eps_norm = 1e-05
F32 = jnp.float32
BF16 = jnp.bfloat16


def dot32(a, b):
    return jnp.dot(a, b, preferred_element_type=F32)


def attention_kernel(
    chunk,
    tokens_hbm,
    state_hbm,
    wq_hbm,
    wk_hbm,
    wd_hbm,
    wv_hbm,
    wg_hbm,
    gain_hbm,
    new_hbm,
    gated_ref,
    tokens,
    state,
    fresh,
    wq,
    wk,
    wd,
    wv,
    wg,
    gain,
    readout,
    in_sem,
    state_sem,
    out_sem,
):
    rows, heads, key_dim, value_dim = state.shape
    chunks = rows // chunk
    small = [
        (tokens_hbm, tokens),
        (wk_hbm, wk),
        (wd_hbm, wd),
        (wq_hbm, wq),
        (wv_hbm, wv),
        (wg_hbm, wg),
        (gain_hbm, gain),
    ]
    copies = [
        pltpu.make_async_copy(src, dst, in_sem.at[n]) for n, (src, dst) in enumerate(small)
    ]
    ins = [
        pltpu.make_async_copy(
            state_hbm.at[pl.ds(n * chunk, chunk)], state.at[pl.ds(n * chunk, chunk)], state_sem.at[n]
        )
        for n in range(chunks)
    ]
    outs = [
        pltpu.make_async_copy(
            fresh.at[pl.ds(n * chunk, chunk)], new_hbm.at[pl.ds(n * chunk, chunk)], out_sem.at[n]
        )
        for n in range(chunks)
    ]
    for n in range(5):
        copies[n].start()
    for one in ins:
        one.start()
    copies[5].start()
    copies[6].start()

    copies[0].wait()
    x = tokens[...]
    copies[1].wait()
    keys = dot32(x, wk[...])
    copies[2].wait()
    pre = dot32(x, wd[...])
    decay = jnp.exp((jnp.minimum(pre, 0.0) - jnp.log1p(jnp.exp(-jnp.abs(pre)))) / 16.0)
    copies[3].wait()
    queries = dot32(x, wq[...]) * key_dim ** (-0.5)
    copies[4].wait()
    values = dot32(x, wv[...])
    columns = []
    for h in range(heads):
        part = slice(h * key_dim, (h + 1) * key_dim)
        pad = jnp.zeros((key_dim - 3 * rows, key_dim), F32)
        stacked = jnp.concatenate([keys[:, part], decay[:, part], queries[:, part], pad], axis=0)
        columns.append(stacked.T)
    for n in range(chunks):
        ins[n].wait()
        for b in range(n * chunk, (n + 1) * chunk):
            for h in range(heads):
                col = columns[h]
                v = values[b : b + 1, h * value_dim : (h + 1) * value_dim]
                new = (
                    col[:, rows + b : rows + b + 1] * state[b, h]
                    + col[:, b : b + 1] * v
                )
                fresh[b, h] = new
                readout[b : b + 1, h * value_dim : (h + 1) * value_dim] = jnp.sum(
                    col[:, 2 * rows + b : 2 * rows + b + 1] * new, axis=0, keepdims=True
                )
        outs[n].start()
    copies[5].wait()
    gate = dot32(x, wg[...])
    copies[6].wait()
    for h in range(heads):
        part = slice(h * value_dim, (h + 1) * value_dim)
        r = readout[:, part]
        scale = lax.rsqrt(jnp.mean(r * r, axis=-1, keepdims=True) + eps_norm)
        gated_ref[:, part] = (r * scale * gain[...] * jax.nn.silu(gate[:, part])).astype(BF16)
    for one in outs:
        one.wait()


def layer_kernel(
    n_ep,
    n_tp,
    cap,
    gated,
    wo_hbm,
    tokens_hbm,
    norm_gain_hbm,
    norm_bias_hbm,
    group_w_hbm,
    router_w_hbm,
    routes_hbm,
    eg_hbm,
    eu_hbm,
    ed_hbm,
    out_ref,
    wo,
    tokens,
    norm_gain,
    norm_bias,
    group_w,
    router_w,
    routes,
    eg,
    eu,
    ed,
    part_mine,
    part_other,
    outgoing,
    arrived,
    results,
    returned,
    stat_mine,
    stat_other,
    in_sem,
    pair_sem,
    stat_sem,
    go_send,
    go_recv,
    back_send,
    back_recv,
):
    me = lax.axis_index("ep")
    core = lax.axis_index("tp")
    rows, width = tokens.shape
    half = width // n_tp
    per_group = router_w.shape[0] // group_w.shape[0]
    slots = n_ep * cap
    operands = [
        (wo_hbm, wo),
        (routes_hbm, routes),
        (tokens_hbm, tokens),
        (norm_gain_hbm, norm_gain),
        (norm_bias_hbm, norm_bias),
        (group_w_hbm, group_w),
        (router_w_hbm, router_w),
        (eg_hbm, eg),
        (eu_hbm, eu),
        (ed_hbm, ed),
    ]
    order = sorted(range(1, n_ep), key=lambda i: abs(2 * i - n_ep))

    def over_peers(body):
        if n_ep <= 32:
            for i in order:
                body(i)
        else:

            def step(i, carry):
                body(i)
                return carry

            lax.fori_loop(1, n_ep, step, 0)

    barrier = pltpu.get_barrier_semaphore()

    def greet(i):
        for c in range(n_tp):
            pl.semaphore_signal(
                barrier, inc=1, device_id=(lax.rem(me + i, n_ep), c), device_id_type=MESH
            )

    loads = [
        pltpu.make_async_copy(src, dst, in_sem.at[n]) for n, (src, dst) in enumerate(operands)
    ]
    for one in loads:
        one.start()
    over_peers(greet)
    for c in range(1, n_tp):
        pl.semaphore_signal(
            barrier, inc=1, device_id=(me, lax.rem(core + c, n_tp)), device_id_type=MESH
        )

    loads[0].wait()
    part_mine[...] = dot32(gated[...], wo[...]).astype(BF16)

    loads[1].wait()
    first, second = routes[0:1, :], routes[1:2, :]
    before = (
        lax.broadcasted_iota(jnp.int32, (rows, rows), 0)
        < lax.broadcasted_iota(jnp.int32, (rows, rows), 1)
    ).astype(BF16)

    def slot_of(count, to_expert):
        line = lax.broadcasted_iota(jnp.int32, (count, rows), 0)
        expert = to_expert(lax.div(line, cap))
        place = lax.rem(line, cap).astype(F32)
        hit0, hit1 = first == expert, second == expert
        either = jnp.where(hit0, 1.0, jnp.where(hit1, 1.0, 0.0))
        earlier = dot32(either.astype(BF16), before)
        placed = jnp.where(earlier == place, 1.0, 0.0)
        return jnp.where(hit0, placed, 0.0), jnp.where(hit1, placed, 0.0)

    send0, send1 = slot_of(slots, lambda j: j * n_tp + core)
    pick_send = (send0 + send1).astype(BF16)
    back0, back1 = slot_of(slots * n_tp, lambda j: j)
    for n in range(2, len(loads)):
        loads[n].wait()
    base = alpha_res * tokens[...].astype(F32) + part_mine[...].astype(F32)

    pl.semaphore_wait(barrier, n_ep * n_tp - 1)
    swap = pltpu.make_async_remote_copy(
        src_ref=part_mine,
        dst_ref=part_other,
        send_sem=pair_sem.at[0],
        recv_sem=pair_sem.at[1],
        device_id=(me, 1 - core),
        device_id_type=MESH,
    )
    swap.start()
    swap.wait()
    mixed = base + part_other[...].astype(F32)
    centered = mixed - jnp.mean(mixed, axis=-1, keepdims=True)
    spread = jnp.mean(centered * centered, axis=-1, keepdims=True)
    hidden = (
        centered * lax.rsqrt(spread + eps_norm) * norm_gain[0:1, :] + norm_bias[0:1, :]
    ).astype(BF16)

    outgoing[...] = dot32(pick_send, hidden).reshape(n_ep, cap, width).astype(BF16)

    def dispatch(i):
        there = lax.rem(me + i, n_ep)
        return pltpu.make_async_remote_copy(
            src_ref=outgoing.at[there],
            dst_ref=arrived.at[me],
            send_sem=go_send.at[i],
            recv_sem=go_recv.at[i],
            device_id=(there, core),
            device_id_type=MESH,
        )

    over_peers(lambda i: dispatch(i).start())
    arrived[me] = outgoing[me]

    across = (((1,), (1,)), ((), ()))
    group_logit = lax.dot_general(group_w[...], hidden, across, preferred_element_type=F32)
    expert_logit = lax.dot_general(router_w[...], hidden, across, preferred_element_type=F32)
    own_group = lax.div(first, per_group)
    group_hit = own_group == lax.broadcasted_iota(jnp.int32, group_logit.shape, 0)
    own_logit = jnp.sum(jnp.where(group_hit, group_logit, 0.0), axis=0, keepdims=True)
    share = 1.0 / jnp.sum(jnp.exp(group_logit - own_logit), axis=0, keepdims=True)
    expert_iota = lax.broadcasted_iota(jnp.int32, expert_logit.shape, 0)
    logit0 = jnp.sum(jnp.where(first == expert_iota, expert_logit, 0.0), axis=0, keepdims=True)
    logit1 = jnp.sum(jnp.where(second == expert_iota, expert_logit, 0.0), axis=0, keepdims=True)
    weighted = back0 * (share * jax.nn.sigmoid(logit0 - logit1)) + back1 * (
        share * jax.nn.sigmoid(logit1 - logit0)
    )
    upper = weighted.astype(BF16)
    lower = (weighted - upper.astype(F32)).astype(BF16)
    mine = jnp.where(core == 0, hidden[:, :half].astype(F32), hidden[:, half:].astype(F32))
    base = alpha_res * mine
    gain = jnp.where(core == 0, norm_gain[1:2, :half], norm_gain[1:2, half:])
    shift = jnp.where(core == 0, norm_bias[1:2, :half], norm_bias[1:2, half:])

    over_peers(lambda i: dispatch(i).wait())
    rows_in = arrived[...].astype(F32).reshape(slots, width).astype(BF16)
    gate_part = dot32(rows_in, eg[0])
    up_part = dot32(rows_in, eu[0])
    activation = (jax.nn.silu(gate_part) * up_part).astype(BF16)

    def send_back(i, c):
        there = lax.rem(me + i, n_ep)
        to = lax.rem(core + c, n_tp)
        return pltpu.make_async_remote_copy(
            src_ref=results.at[c, there],
            dst_ref=returned.at[me * n_tp + core],
            send_sem=back_send.at[c, i],
            recv_sem=back_recv.at[c, i],
            device_id=(there, to),
            device_id_type=MESH,
        )

    for c in range(n_tp):
        start = pl.multiple_of(lax.rem(core + c, n_tp) * half, half)
        result = dot32(activation, ed[0, :, pl.ds(start, half)])
        results[c] = result.reshape(n_ep, cap, half).astype(BF16)
        over_peers(lambda i: send_back(i, c).start())
        if c:
            send_back(0, c).start()
    returned[me * n_tp + core] = results[0, me]

    def home(i):
        for c in range(n_tp):
            send_back(i, c).wait()

    over_peers(home)
    for c in range(1, n_tp):
        send_back(0, c).wait()
    fetched = returned[...].astype(F32).reshape(slots * n_tp, half).astype(BF16)
    down = (((0,), (0,)), ((), ()))
    blended = (
        base
        + lax.dot_general(upper, fetched, down, preferred_element_type=F32)
        + lax.dot_general(lower, fetched, down, preferred_element_type=F32)
    )
    total = jnp.sum(blended, axis=1, keepdims=True)
    squares = jnp.sum(blended * blended, axis=1, keepdims=True)
    lane = lax.broadcasted_iota(jnp.int32, stat_mine.shape, 1)
    stats = jnp.where(lane == 0, total, squares)
    stat_mine[...] = stats
    trade = pltpu.make_async_remote_copy(
        src_ref=stat_mine,
        dst_ref=stat_other,
        send_sem=stat_sem.at[0],
        recv_sem=stat_sem.at[1],
        device_id=(me, 1 - core),
        device_id_type=MESH,
    )
    trade.start()
    trade.wait()
    both = stats + stat_other[...]
    row_mean = both[:, 0:1] / width
    spread = both[:, 1:2] / width - row_mean * row_mean
    out_ref[...] = (
        (blended - row_mean) * lax.rsqrt(spread + eps_norm) * gain + shift
    ).astype(BF16)


def on_device(
    n_ep,
    n_tp,
    tokens,
    recurrent_state,
    query_weight,
    key_weight,
    decay_weight,
    value_weight,
    gate_weight,
    head_gain,
    output_weight,
    norm_gain,
    norm_bias,
    group_router,
    router_weight,
    routes,
    expert_gate,
    expert_up,
    expert_down,
):
    rows, width = tokens.shape
    heads, key_dim, value_dim = recurrent_state.shape[1:]
    in_hbm = pl.BlockSpec(memory_space=pltpu.HBM)
    vmem = pl.BlockSpec(memory_space=pltpu.VMEM)
    chunk = 4
    chunks = rows // chunk
    dma = pltpu.SemaphoreType.DMA

    def like(a):
        return pltpu.VMEM(a.shape, a.dtype)

    def pinned(arrays):
        return tuple(pltpu.with_memory_space_constraint(a, pltpu.HBM) for a in arrays)

    gain_row = head_gain.reshape(1, value_dim)
    new_state, gated = pl.pallas_call(
        functools.partial(attention_kernel, chunk),
        out_shape=(
            jax.ShapeDtypeStruct(recurrent_state.shape, F32),
            jax.ShapeDtypeStruct((rows, heads * value_dim), BF16),
        ),
        in_specs=[in_hbm] * 8,
        out_specs=(in_hbm, vmem),
        scratch_shapes=[
            like(tokens),
            like(recurrent_state),
            like(recurrent_state),
            like(query_weight),
            like(key_weight),
            like(decay_weight),
            like(value_weight),
            like(gate_weight),
            like(gain_row),
            pltpu.VMEM((rows, heads * value_dim), F32),
            dma((7,)),
            dma((chunks,)),
            dma((chunks,)),
        ],
        compiler_params=pltpu.CompilerParams(vmem_limit_bytes=40 * 1024 * 1024),
        name="attention",
    )(
        *pinned(
            (
                tokens,
                recurrent_state,
                query_weight,
                key_weight,
                decay_weight,
                value_weight,
                gate_weight,
                gain_row,
            )
        )
    )
    experts = router_weight.shape[1]
    cap = 2 * max(1, rows // experts)
    half = width // n_tp
    operands = (
        output_weight,
        tokens,
        norm_gain,
        norm_bias,
        group_router.T,
        router_weight.T,
        routes.T,
        expert_gate,
        expert_up,
        expert_down,
    )
    new_tokens = pl.pallas_call(
        functools.partial(layer_kernel, n_ep, n_tp, cap),
        out_shape=jax.ShapeDtypeStruct((rows, half), BF16),
        in_specs=[vmem] + [in_hbm] * len(operands),
        out_specs=vmem,
        scratch_shapes=[like(a) for a in operands]
        + [
            pltpu.VMEM((rows, width), BF16),
            pltpu.VMEM((rows, width), BF16),
            pltpu.VMEM((n_ep, cap, width), BF16),
            pltpu.VMEM((n_ep, cap, width), BF16),
            pltpu.VMEM((n_tp, n_ep, cap, half), BF16),
            pltpu.VMEM((n_ep * n_tp, cap, half), BF16),
            pltpu.VMEM((rows, 128), F32),
            pltpu.VMEM((rows, 128), F32),
            dma((len(operands),)),
            dma((2,)),
            dma((2,)),
            dma((n_ep,)),
            dma((n_ep,)),
            dma((n_tp, n_ep)),
            dma((n_tp, n_ep)),
        ],
        compiler_params=pltpu.CompilerParams(
            collective_id=0, has_side_effects=True, vmem_limit_bytes=40 * 1024 * 1024
        ),
        name="layer",
    )(gated, *pinned(operands))
    return new_tokens, new_state


def solution(mesh):
    in_specs = (
        P("ep", None),
        P("ep", "tp", None, None),
        P(None, "tp"),
        P(None, "tp"),
        P(None, "tp"),
        P(None, "tp"),
        P(None, "tp"),
        P(),
        P("tp", None),
        P(),
        P(),
        P(),
        P(),
        P("ep", None),
        P(("ep", "tp"), None, None),
        P(("ep", "tp"), None, None),
        P(("ep", "tp"), None, None),
    )
    out_specs = (P("ep", "tp"), P("ep", "tp", None, None))
    return jax.shard_map(
        functools.partial(on_device, mesh.shape["ep"], mesh.shape["tp"]),
        mesh=mesh,
        in_specs=in_specs,
        out_specs=out_specs,
        check_vma=False,
    )
```

profile of v0, /device:TPU:0, one launch (start us, length us, event | category | flops | bytes accessed | tf_op | source)
XLA Modules:
  0.0 30.4 jit_solution(1792134325441759081)
XLA Ops:
  0.6 6.5 %attention.1 = (f32[16,2,128,256]{3,2,1,0:T(8,128)}, bf16[16,512]{1,0:T(8,128)(2,1)S(1)}) custom-call(bf16[16,2048]{1,0:T(8,128)(2,1)} %tokens_hbm.3, f32[16,2,128,256]{3,2,1,0:T(8,128)} %state_hbm.1, bf16[2048,256]{1,0:T(8,128)(2,1)} %wq_hbm.1, bf16[2048,256]{1,0:T(8,128)(2,1)} %wk_hbm.1, bf16[2048,256]{1,0:T(8,128)(2,1)} %wd_hbm.1, ...), custom_call_target="tpu_custom_call" | custom-call | tf_op jit(solution)/shard_map/attention/pallas_call | solution.py:398
  7.1 22.6 %layer.1 = bf16[16,1024]{1,0:T(8,128)(2,1)S(1)} custom-call(bf16[16,512]{1,0:T(8,128)(2,1)S(1)} %get-tuple-element.4.gated, bf16[512,2048]{1,0:T(8,128)(2,1)} %wo_hbm.1, bf16[16,2048]{1,0:T(8,128)(2,1)} %tokens_hbm.3, f32[2,2048]{1,0:T(2,128)} %norm_gain_hbm.1, f32[2,2048]{1,0:T(2,128)} %norm_bias_hbm.1, bf16[4,2048]{1,0:T(4,128)(2,1)} %bitcast.5, ...), custom_call_target="tpu_custom_call" | custom-call | tf_op jit(solution)/shard_map/layer/pallas_call | solution.py:452
  29.7 0.6 %copy.20 = bf16[16,1024]{1,0:T(8,128)(2,1)} copy(bf16[16,1024]{1,0:T(8,128)(2,1)S(1)} %layer.1) | data formatting | bytes 65536
where the time goes:
time: 30.5 us; the launch traced here: 30.4 us
  Pallas kernels  29.1 us (95%)
  between operations  0.65 us (2%)
  local copies, waits for them, and re-layouts  0.62 us (2%)
    pallas_call x1, Pallas kernels, on_device(): pl.pallas_call(functools.partial(layer_kernel, n_ep, n_tp, cap), out_shap...  22.6 us
    pallas_call x1, Pallas kernels, on_device(): pl.pallas_call(functools.partial(attention_kernel, chunk), out_shape=(jax...  6.46 us
    unnamed x1, local copies, waits for them, and re-layouts  0.62 us

commit v1 on v0

v1 whole, which is shorter than its diff:
```python
import functools

import jax
import jax.numpy as jnp
from jax import lax
from jax.experimental import pallas as pl
from jax.experimental.pallas import tpu as pltpu
from jax.sharding import PartitionSpec as P

MESH = pl.DeviceIdType.MESH
alpha_res = 2.0**0.5
eps_norm = 1e-05
F32 = jnp.float32
BF16 = jnp.bfloat16


def dot32(a, b):
    return jnp.dot(a, b, preferred_element_type=F32)


def layer_kernel(
    n_ep,
    n_tp,
    cap,
    chunk,
    tokens_hbm,
    state_hbm,
    wq_hbm,
    wk_hbm,
    wd_hbm,
    wv_hbm,
    wg_hbm,
    gain_hbm,
    wo_hbm,
    norm_gain_hbm,
    norm_bias_hbm,
    group_w_hbm,
    router_w_hbm,
    routes_hbm,
    eg_hbm,
    eu_hbm,
    ed_hbm,
    out_ref,
    fresh,
    tokens,
    state,
    wq,
    wk,
    wd,
    wv,
    wg,
    head_gain,
    wo,
    norm_gain,
    norm_bias,
    group_w,
    router_w,
    routes,
    eg,
    eu,
    ed,
    readout,
    part_mine,
    part_other,
    outgoing,
    arrived,
    results,
    returned,
    stat_mine,
    stat_other,
    in_sem,
    state_sem,
    pair_sem,
    stat_sem,
    go_send,
    go_recv,
    back_send,
    back_recv,
):
    me = lax.axis_index("ep")
    core = lax.axis_index("tp")
    rows, width = tokens.shape
    heads, key_dim, value_dim = state.shape[1:]
    half = width // n_tp
    per_group = router_w.shape[0] // group_w.shape[0]
    slots = n_ep * cap
    chunks = rows // chunk
    unrolled = n_ep <= 32

    def peer(i):
        if not unrolled or n_ep & (n_ep - 1):
            return lax.rem(me + i, n_ep)
        there = me
        bit = 1
        while bit < n_ep:
            if i & bit:
                there = there + bit * (1 - 2 * lax.rem(lax.div(me, bit), 2))
            bit *= 2
        return there

    order = sorted(range(1, n_ep), key=lambda i: -((i & 1) + (i >> 1 & 1) + (i >> 2)))

    def over_peers(body):
        if unrolled:
            for i in order:
                body(i)
        else:

            def step(i, carry):
                body(i)
                return carry

            lax.fori_loop(1, n_ep, step, 0)

    names = (
        ("routes", routes_hbm, routes),
        ("tokens", tokens_hbm, tokens),
        ("wk", wk_hbm, wk),
        ("wd", wd_hbm, wd),
        ("wq", wq_hbm, wq),
        ("wv", wv_hbm, wv),
        ("wg", wg_hbm, wg),
        ("head_gain", gain_hbm, head_gain),
        ("wo", wo_hbm, wo),
        ("norm_gain", norm_gain_hbm, norm_gain),
        ("norm_bias", norm_bias_hbm, norm_bias),
        ("group_w", group_w_hbm, group_w),
        ("router_w", router_w_hbm, router_w),
        ("eg", eg_hbm, eg),
        ("eu", eu_hbm, eu),
        ("ed", ed_hbm, ed),
    )
    load = {
        name: pltpu.make_async_copy(src, dst, in_sem.at[n])
        for n, (name, src, dst) in enumerate(names)
    }
    ins = [
        pltpu.make_async_copy(
            state_hbm.at[pl.ds(n * chunk, chunk)], state.at[pl.ds(n * chunk, chunk)], state_sem.at[n]
        )
        for n in range(chunks)
    ]
    for name in ("routes", "tokens", "wk", "wd", "wq", "wv"):
        load[name].start()
    for one in ins:
        one.start()
    for name in ("wg", "head_gain", "wo", "norm_gain", "norm_bias", "group_w", "router_w"):
        load[name].start()

    barrier = pltpu.get_barrier_semaphore()

    def greet(i):
        for c in range(n_tp):
            pl.semaphore_signal(barrier, inc=1, device_id=(peer(i), c), device_id_type=MESH)

    over_peers(greet)
    for c in range(1, n_tp):
        pl.semaphore_signal(
            barrier, inc=1, device_id=(me, lax.rem(core + c, n_tp)), device_id_type=MESH
        )

    load["routes"].wait()
    first, second = routes[0:1, :], routes[1:2, :]
    before = (
        lax.broadcasted_iota(jnp.int32, (rows, rows), 0)
        < lax.broadcasted_iota(jnp.int32, (rows, rows), 1)
    ).astype(BF16)

    def slot_of(count, to_expert):
        line = lax.broadcasted_iota(jnp.int32, (count, rows), 0)
        expert = to_expert(lax.div(line, cap))
        place = lax.rem(line, cap).astype(F32)
        hit0, hit1 = first == expert, second == expert
        either = jnp.where(hit0, 1.0, jnp.where(hit1, 1.0, 0.0))
        earlier = dot32(either.astype(BF16), before)
        placed = jnp.where(earlier == place, 1.0, 0.0)
        return jnp.where(hit0, placed, 0.0), jnp.where(hit1, placed, 0.0)

    send0, send1 = slot_of(slots, lambda j: j * n_tp + core)
    pick_send = (send0 + send1).astype(BF16)
    back0, back1 = slot_of(slots * n_tp, lambda j: j)

    load["tokens"].wait()
    x = tokens[...]
    load["wk"].wait()
    keys = dot32(x, wk[...])
    load["wd"].wait()
    pre = dot32(x, wd[...])
    decay = jnp.exp((jnp.minimum(pre, 0.0) - jnp.log1p(jnp.exp(-jnp.abs(pre)))) / 16.0)
    load["wq"].wait()
    queries = dot32(x, wq[...]) * key_dim ** (-0.5)
    load["wv"].wait()
    values = dot32(x, wv[...])
    columns = []
    for h in range(heads):
        part = slice(h * key_dim, (h + 1) * key_dim)
        pad = jnp.zeros((key_dim - 3 * rows, key_dim), F32)
        stacked = jnp.concatenate([keys[:, part], decay[:, part], queries[:, part], pad], axis=0)
        columns.append(stacked.T)
    for n in range(chunks):
        ins[n].wait()
        for b in range(n * chunk, (n + 1) * chunk):
            for h in range(heads):
                col = columns[h]
                v = values[b : b + 1, h * value_dim : (h + 1) * value_dim]
                new = (
                    col[:, rows + b : rows + b + 1] * state[b, h]
                    + col[:, b : b + 1] * v
                )
                fresh[b, h] = new
                readout[b : b + 1, h * value_dim : (h + 1) * value_dim] = jnp.sum(
                    col[:, 2 * rows + b : 2 * rows + b + 1] * new, axis=0, keepdims=True
                )
    for name in ("eg", "eu", "ed"):
        load[name].start()
    load["wg"].wait()
    gate = dot32(x, wg[...])
    load["head_gain"].wait()
    gated = []
    for h in range(heads):
        part = slice(h * value_dim, (h + 1) * value_dim)
        r = readout[:, part]
        scale = lax.rsqrt(jnp.mean(r * r, axis=-1, keepdims=True) + eps_norm)
        gated.append((r * scale * head_gain[...] * jax.nn.silu(gate[:, part])).astype(BF16))
    load["wo"].wait()
    part_mine[...] = dot32(jnp.concatenate(gated, axis=1), wo[...]).astype(BF16)

    pl.semaphore_wait(barrier, n_ep * n_tp - 1)
    swap = pltpu.make_async_remote_copy(
        src_ref=part_mine,
        dst_ref=part_other,
        send_sem=pair_sem.at[0],
        recv_sem=pair_sem.at[1],
        device_id=(me, 1 - core),
        device_id_type=MESH,
    )
    swap.start()
    for name in ("norm_gain", "norm_bias", "group_w", "router_w"):
        load[name].wait()
    base = alpha_res * tokens[...].astype(F32) + part_mine[...].astype(F32)
    swap.wait()
    mixed = base + part_other[...].astype(F32)
    centered = mixed - jnp.mean(mixed, axis=-1, keepdims=True)
    spread = jnp.mean(centered * centered, axis=-1, keepdims=True)
    hidden = (
        centered * lax.rsqrt(spread + eps_norm) * norm_gain[0:1, :] + norm_bias[0:1, :]
    ).astype(BF16)

    outgoing[...] = dot32(pick_send, hidden).reshape(n_ep, cap, width).astype(BF16)

    def dispatch(i):
        there = peer(i)
        return pltpu.make_async_remote_copy(
            src_ref=outgoing.at[there],
            dst_ref=arrived.at[me],
            send_sem=go_send.at[i],
            recv_sem=go_recv.at[i],
            device_id=(there, core),
            device_id_type=MESH,
        )

    over_peers(lambda i: dispatch(i).start())
    arrived[me] = outgoing[me]

    across = (((1,), (1,)), ((), ()))
    group_logit = lax.dot_general(group_w[...], hidden, across, preferred_element_type=F32)
    expert_logit = lax.dot_general(router_w[...], hidden, across, preferred_element_type=F32)
    own_group = lax.div(first, per_group)
    group_hit = own_group == lax.broadcasted_iota(jnp.int32, group_logit.shape, 0)
    own_logit = jnp.sum(jnp.where(group_hit, group_logit, 0.0), axis=0, keepdims=True)
    share = 1.0 / jnp.sum(jnp.exp(group_logit - own_logit), axis=0, keepdims=True)
    expert_iota = lax.broadcasted_iota(jnp.int32, expert_logit.shape, 0)
    logit0 = jnp.sum(jnp.where(first == expert_iota, expert_logit, 0.0), axis=0, keepdims=True)
    logit1 = jnp.sum(jnp.where(second == expert_iota, expert_logit, 0.0), axis=0, keepdims=True)
    weighted = back0 * (share * jax.nn.sigmoid(logit0 - logit1)) + back1 * (
        share * jax.nn.sigmoid(logit1 - logit0)
    )
    upper = weighted.astype(BF16)
    lower = (weighted - upper.astype(F32)).astype(BF16)
    mine = jnp.where(core == 0, hidden[:, :half].astype(F32), hidden[:, half:].astype(F32))
    base = alpha_res * mine
    gain = jnp.where(core == 0, norm_gain[1:2, :half], norm_gain[1:2, half:])
    shift = jnp.where(core == 0, norm_bias[1:2, :half], norm_bias[1:2, half:])
    for name in ("eg", "eu", "ed"):
        load[name].wait()

    over_peers(lambda i: dispatch(i).wait())
    rows_in = arrived[...].astype(F32).reshape(slots, width).astype(BF16)
    gate_part = dot32(rows_in, eg[0])
    up_part = dot32(rows_in, eu[0])
    activation = (jax.nn.silu(gate_part) * up_part).astype(BF16)

    def send_back(i, c, from_core):
        there = peer(i)
        return pltpu.make_async_remote_copy(
            src_ref=results.at[c, there],
            dst_ref=returned.at[me * n_tp + core],
            send_sem=back_send.at[c, i],
            recv_sem=back_recv.at[from_core, i],
            device_id=(there, c),
            device_id_type=MESH,
        )

    for c in range(n_tp):
        result = dot32(activation, ed[0, :, c * half : (c + 1) * half])
        results[c] = result.reshape(n_ep, cap, half).astype(BF16)
        over_peers(lambda i: send_back(i, c, core).start())
    beside = pltpu.make_async_remote_copy(
        src_ref=results.at[1 - core, me],
        dst_ref=returned.at[me * n_tp + core],
        send_sem=back_send.at[0, 0],
        recv_sem=back_recv.at[0, 0],
        device_id=(me, 1 - core),
        device_id_type=MESH,
    )
    beside.start()
    returned[me * n_tp + core] = results[core, me]

    def home(i):
        for c in range(n_tp):
            send_back(i, c, c).wait()

    over_peers(home)
    beside.wait()
    fetched = returned[...].astype(F32).reshape(slots * n_tp, half).astype(BF16)
    down = (((0,), (0,)), ((), ()))
    blended = (
        base
        + lax.dot_general(upper, fetched, down, preferred_element_type=F32)
        + lax.dot_general(lower, fetched, down, preferred_element_type=F32)
    )
    total = jnp.sum(blended, axis=1, keepdims=True)
    squares = jnp.sum(blended * blended, axis=1, keepdims=True)
    lane = lax.broadcasted_iota(jnp.int32, stat_mine.shape, 1)
    stats = jnp.where(lane == 0, total, squares)
    stat_mine[...] = stats
    trade = pltpu.make_async_remote_copy(
        src_ref=stat_mine,
        dst_ref=stat_other,
        send_sem=stat_sem.at[0],
        recv_sem=stat_sem.at[1],
        device_id=(me, 1 - core),
        device_id_type=MESH,
    )
    trade.start()
    trade.wait()
    both = stats + stat_other[...]
    row_mean = both[:, 0:1] / width
    spread = both[:, 1:2] / width - row_mean * row_mean
    out_ref[...] = (
        (blended - row_mean) * lax.rsqrt(spread + eps_norm) * gain + shift
    ).astype(BF16)


def store_kernel(chunk, out_ref, fresh, out_hbm, new_hbm, out_sem, new_sem):
    copies = [pltpu.make_async_copy(out_ref, out_hbm, out_sem)]
    for n in range(fresh.shape[0] // chunk):
        part = pl.ds(n * chunk, chunk)
        copies.append(pltpu.make_async_copy(fresh.at[part], new_hbm.at[part], new_sem.at[n]))
    for one in copies:
        one.start()
    for one in copies:
        one.wait()


def on_device(
    n_ep,
    n_tp,
    tokens,
    recurrent_state,
    query_weight,
    key_weight,
    decay_weight,
    value_weight,
    gate_weight,
    head_gain,
    output_weight,
    norm_gain,
    norm_bias,
    group_router,
    router_weight,
    routes,
    expert_gate,
    expert_up,
    expert_down,
):
    rows, width = tokens.shape
    heads, key_dim, value_dim = recurrent_state.shape[1:]
    in_hbm = pl.BlockSpec(memory_space=pltpu.HBM)
    vmem = pl.BlockSpec(memory_space=pltpu.VMEM)
    chunk = 4
    chunks = rows // chunk
    dma = pltpu.SemaphoreType.DMA

    def like(a):
        return pltpu.VMEM(a.shape, a.dtype)

    def pinned(arrays):
        return tuple(pltpu.with_memory_space_constraint(a, pltpu.HBM) for a in arrays)

    experts = router_weight.shape[1]
    cap = 2 * max(1, rows // experts)
    half = width // n_tp
    operands = (
        tokens,
        recurrent_state,
        query_weight,
        key_weight,
        decay_weight,
        value_weight,
        gate_weight,
        head_gain.reshape(1, value_dim),
        output_weight,
        norm_gain,
        norm_bias,
        group_router.T,
        router_weight.T,
        routes.T,
        expert_gate,
        expert_up,
        expert_down,
    )
    new_tokens, new_state = pl.pallas_call(
        functools.partial(layer_kernel, n_ep, n_tp, cap, chunk),
        out_shape=(
            jax.ShapeDtypeStruct((rows, half), BF16),
            jax.ShapeDtypeStruct(recurrent_state.shape, F32),
        ),
        in_specs=[in_hbm] * len(operands),
        out_specs=(vmem, vmem),
        scratch_shapes=[like(a) for a in operands]
        + [
            pltpu.VMEM((rows, heads * value_dim), F32),
            pltpu.VMEM((rows, width), BF16),
            pltpu.VMEM((rows, width), BF16),
            pltpu.VMEM((n_ep, cap, width), BF16),
            pltpu.VMEM((n_ep, cap, width), BF16),
            pltpu.VMEM((n_tp, n_ep, cap, half), BF16),
            pltpu.VMEM((n_ep * n_tp, cap, half), BF16),
            pltpu.VMEM((rows, 128), F32),
            pltpu.VMEM((rows, 128), F32),
            dma((len(operands) - 1,)),
            dma((chunks,)),
            dma((2,)),
            dma((2,)),
            dma((n_ep,)),
            dma((n_ep,)),
            dma((n_tp, n_ep)),
            dma((n_tp, n_ep)),
        ],
        compiler_params=pltpu.CompilerParams(
            collective_id=0, has_side_effects=True, vmem_limit_bytes=40 * 1024 * 1024
        ),
        name="layer",
    )(*pinned(operands))
    return pl.pallas_call(
        functools.partial(store_kernel, chunk),
        out_shape=(
            jax.ShapeDtypeStruct(new_tokens.shape, BF16),
            jax.ShapeDtypeStruct(new_state.shape, F32),
        ),
        in_specs=[vmem, vmem],
        out_specs=(in_hbm, in_hbm),
        scratch_shapes=[dma, dma((chunks,))],
        compiler_params=pltpu.CompilerParams(vmem_limit_bytes=8 * 1024 * 1024),
        name="store",
    )(new_tokens, new_state)


def solution(mesh):
    in_specs = (
        P("ep", None),
        P("ep", "tp", None, None),
        P(None, "tp"),
        P(None, "tp"),
        P(None, "tp"),
        P(None, "tp"),
        P(None, "tp"),
        P(),
        P("tp", None),
        P(),
        P(),
        P(),
        P(),
        P("ep", None),
        P(("ep", "tp"), None, None),
        P(("ep", "tp"), None, None),
        P(("ep", "tp"), None, None),
    )
    out_specs = (P("ep", "tp"), P("ep", "tp", None, None))
    return jax.shard_map(
        functools.partial(on_device, mesh.shape["ep"], mesh.shape["tp"]),
        mesh=mesh,
        in_specs=in_specs,
        out_specs=out_specs,
        check_vma=False,
    )
```

time: 30.5 us -> 28 us (0.918)
  Pallas kernels: 29.1 us -> 27.2 us
  local copies, waits for them, and re-layouts: 0.62 us -> 0 us
    pallas_call x2, Pallas kernels: 29.1 us -> 27.2 us  [the longest x1 25.1 us: on_device(): pl.pallas_call(functools.partial(layer_kernel, n_ep, n_tp, cap, chunk), o...]
    unnamed x1 -> x0, local copies, waits for them, and re-layouts: 0.62 us -> none
where the time goes in v1:
time: 28 us; the launch traced here: 27.8 us
  Pallas kernels  27.2 us (97%)
  between operations  0.65 us (2%)
    pallas_call x1, Pallas kernels, on_device(): pl.pallas_call(functools.partial(layer_kernel, n_ep, n_tp, cap, chunk), o...  25.1 us
    pallas_call x1, Pallas kernels, on_device(): pl.pallas_call(functools.partial(store_kernel, chunk), out_shape=(jax.Sha...  2.06 us

profile of v1, /device:TPU:0, one launch (start us, length us, event | category | flops | bytes accessed | tf_op | source)
XLA Modules:
  0.0 27.8 jit_solution(11857020492975193092)
XLA Ops:
  0.6 25.1 %layer.1 = (bf16[16,1024]{1,0:T(8,128)(2,1)S(1)}, f32[16,2,128,256]{3,2,1,0:T(8,128)S(1)}) custom-call(bf16[16,2048]{1,0:T(8,128)(2,1)} %tokens_hbm.1, f32[16,2,128,256]{3,2,1,0:T(8,128)} %state_hbm.1, bf16[2048,256]{1,0:T(8,128)(2,1)} %wq_hbm.1, bf16[2048,256]{1,0:T(8,128)(2,1)} %wk_hbm.1, bf16[2048,256]{1,0:T(8,128)(2,1)} %wd_hbm.1, ...), custom_call_target="tpu_custom_call" | custom-call | tf_op jit(solution)/shard_map/layer/pallas_call | solution.py:423
  25.8 2.1 %store.1 = (bf16[16,1024]{1,0:T(8,128)(2,1)}, f32[16,2,128,256]{3,2,1,0:T(8,128)}) custom-call(bf16[16,1024]{1,0:T(8,128)(2,1)S(1)} %get-tuple-element.4.out_ref, f32[16,2,128,256]{3,2,1,0:T(8,128)S(1)} %get-tuple-element.5.fresh), custom_call_target="tpu_custom_call" | custom-call | tf_op jit(solution)/shard_map/store/pallas_call | solution.py:456

commit v2 on v1

--- a/solution.py
+++ b/solution.py
@@ -1,4 +1,5 @@
 import functools
+import math
 
 import jax
 import jax.numpy as jnp
@@ -12,10 +13,22 @@
 eps_norm = 1e-05
 F32 = jnp.float32
 BF16 = jnp.bfloat16
+PIECE = 128 * 1024
+AHEAD = 8 * 1024 * 1024
 
 
 def dot32(a, b):
     return jnp.dot(a, b, preferred_element_type=F32)
+
+
+def pieces(shape, dtype, size=PIECE):
+    lead = 1 if len(shape) > 2 and shape[0] == 1 else 0
+    whole = math.prod(shape) * jnp.dtype(dtype).itemsize
+    count = max(1, min(whole // size, shape[lead] // (16 if len(shape) - lead == 2 else 1)))
+    while shape[lead] % count:
+        count -= 1
+    step = shape[lead] // count
+    return [(0,) * lead + (pl.ds(n * step, step),) for n in range(count)]
 
 
 def layer_kernel(
@@ -130,22 +143,33 @@
         ("eu", eu_hbm, eu),
         ("ed", ed_hbm, ed),
     )
-    load = {
-        name: pltpu.make_async_copy(src, dst, in_sem.at[n])
-        for n, (name, src, dst) in enumerate(names)
-    }
-    ins = [
-        pltpu.make_async_copy(
-            state_hbm.at[pl.ds(n * chunk, chunk)], state.at[pl.ds(n * chunk, chunk)], state_sem.at[n]
-        )
-        for n in range(chunks)
-    ]
-    for name in ("routes", "tokens", "wk", "wd", "wq", "wv"):
-        load[name].start()
-    for one in ins:
-        one.start()
-    for name in ("wg", "head_gain", "wo", "norm_gain", "norm_bias", "group_w", "router_w"):
-        load[name].start()
+    load = {name: (src, dst, in_sem.at[n]) for n, (name, src, dst) in enumerate(names)}
+    for n in range(chunks):
+        part = pl.ds(n * chunk, chunk)
+        load[n] = (state_hbm.at[part], state.at[part], state_sem.at[n])
+
+    def fetch(name):
+        src, dst, sem = load[name]
+        for part in pieces(src.shape, src.dtype):
+            pltpu.make_async_copy(src.at[part], dst.at[part], sem).start()
+
+    def ready(name):
+        pltpu.make_async_copy(*load[name]).wait()
+        flying.pop(name)
+        fetch_more()
+
+    queue = [*("routes", "tokens", "wd", "wq"), *range(chunks), *("wk", "wv", "head_gain", "wg")]
+    queue += ["wo", "norm_gain", "norm_bias", "group_w", "router_w", "eg", "eu", "ed"]
+    flying = {}
+
+    def fetch_more():
+        while queue and sum(flying.values()) < AHEAD:
+            name = queue.pop(0)
+            src = load[name][0]
+            flying[name] = math.prod(src.shape) * jnp.dtype(src.dtype).itemsize
+            fetch(name)
+
+    fetch_more()
 
     barrier = pltpu.get_barrier_semaphore()
 
@@ -159,7 +183,7 @@
             barrier, inc=1, device_id=(me, lax.rem(core + c, n_tp)), device_id_type=MESH
         )
 
-    load["routes"].wait()
+    ready("routes")
     first, second = routes[0:1, :], routes[1:2, :]
     before = (
         lax.broadcasted_iota(jnp.int32, (rows, rows), 0)
@@ -180,49 +204,46 @@
     pick_send = (send0 + send1).astype(BF16)
     back0, back1 = slot_of(slots * n_tp, lambda j: j)
 
-    load["tokens"].wait()
+    ready("tokens")
     x = tokens[...]
-    load["wk"].wait()
-    keys = dot32(x, wk[...])
-    load["wd"].wait()
+    ready("wd")
     pre = dot32(x, wd[...])
     decay = jnp.exp((jnp.minimum(pre, 0.0) - jnp.log1p(jnp.exp(-jnp.abs(pre)))) / 16.0)
-    load["wq"].wait()
+    ready("wq")
     queries = dot32(x, wq[...]) * key_dim ** (-0.5)
-    load["wv"].wait()
-    values = dot32(x, wv[...])
-    columns = []
-    for h in range(heads):
-        part = slice(h * key_dim, (h + 1) * key_dim)
-        pad = jnp.zeros((key_dim - 3 * rows, key_dim), F32)
-        stacked = jnp.concatenate([keys[:, part], decay[:, part], queries[:, part], pad], axis=0)
-        columns.append(stacked.T)
+    decayed = queries * decay
+
+    def as_columns(parts):
+        pad = jnp.zeros((key_dim - len(parts) * rows, key_dim), F32)
+        return [
+            jnp.concatenate([p[:, h * key_dim : (h + 1) * key_dim] for p in parts] + [pad], axis=0).T
+            for h in range(heads)
+        ]
+
+    reading = as_columns([decayed])
     for n in range(chunks):
-        ins[n].wait()
+        ready(n)
         for b in range(n * chunk, (n + 1) * chunk):
             for h in range(heads):
-                col = columns[h]
-                v = values[b : b + 1, h * value_dim : (h + 1) * value_dim]
-                new = (
-                    col[:, rows + b : rows + b + 1] * state[b, h]
-                    + col[:, b : b + 1] * v
+                readout[b : b + 1, h * value_dim : (h + 1) * value_dim] = jnp.sum(
+                    reading[h][:, b : b + 1] * state[b, h], axis=0, keepdims=True
                 )
-                fresh[b, h] = new
-                readout[b : b + 1, h * value_dim : (h + 1) * value_dim] = jnp.sum(
-                    col[:, 2 * rows + b : 2 * rows + b + 1] * new, axis=0, keepdims=True
-                )
-    for name in ("eg", "eu", "ed"):
-        load[name].start()
-    load["wg"].wait()
+    ready("wk")
+    keys = dot32(x, wk[...])
+    ready("wv")
+    values = dot32(x, wv[...])
+    both = queries * keys
+    ready("wg")
     gate = dot32(x, wg[...])
-    load["head_gain"].wait()
+    ready("head_gain")
     gated = []
     for h in range(heads):
         part = slice(h * value_dim, (h + 1) * value_dim)
-        r = readout[:, part]
+        meet = jnp.sum(both[:, h * key_dim : (h + 1) * key_dim], axis=-1, keepdims=True)
+        r = readout[:, part] + meet * values[:, part]
         scale = lax.rsqrt(jnp.mean(r * r, axis=-1, keepdims=True) + eps_norm)
         gated.append((r * scale * head_gain[...] * jax.nn.silu(gate[:, part])).astype(BF16))
-    load["wo"].wait()
+    ready("wo")
     part_mine[...] = dot32(jnp.concatenate(gated, axis=1), wo[...]).astype(BF16)
 
     pl.semaphore_wait(barrier, n_ep * n_tp - 1)
@@ -236,7 +257,7 @@
     )
     swap.start()
     for name in ("norm_gain", "norm_bias", "group_w", "router_w"):
-        load[name].wait()
+        ready(name)
     base = alpha_res * tokens[...].astype(F32) + part_mine[...].astype(F32)
     swap.wait()
     mixed = base + part_other[...].astype(F32)
@@ -253,14 +274,30 @@
         return pltpu.make_async_remote_copy(
             src_ref=outgoing.at[there],
             dst_ref=arrived.at[me],
-            send_sem=go_send.at[i],
-            recv_sem=go_recv.at[i],
+            send_sem=go_send,
+            recv_sem=go_recv,
             device_id=(there, core),
             device_id_type=MESH,
         )
 
+    others = pl.ds(0, n_ep - 1)
+    all_out = pltpu.make_async_remote_copy(
+        src_ref=outgoing.at[others],
+        dst_ref=arrived.at[others],
+        send_sem=go_send,
+        recv_sem=go_recv,
+        device_id=(peer(1), core),
+        device_id_type=MESH,
+    )
     over_peers(lambda i: dispatch(i).start())
     arrived[me] = outgoing[me]
+
+    columns = as_columns([keys, decay])
+    for b in range(rows):
+        for h in range(heads):
+            col = columns[h]
+            v = values[b : b + 1, h * value_dim : (h + 1) * value_dim]
+            fresh[b, h] = col[:, rows + b : rows + b + 1] * state[b, h] + col[:, b : b + 1] * v
 
     across = (((1,), (1,)), ((), ()))
     group_logit = lax.dot_general(group_w[...], hidden, across, preferred_element_type=F32)
@@ -282,46 +319,47 @@
     gain = jnp.where(core == 0, norm_gain[1:2, :half], norm_gain[1:2, half:])
     shift = jnp.where(core == 0, norm_bias[1:2, :half], norm_bias[1:2, half:])
     for name in ("eg", "eu", "ed"):
-        load[name].wait()
-
-    over_peers(lambda i: dispatch(i).wait())
+        ready(name)
+
+    all_out.wait()
     rows_in = arrived[...].astype(F32).reshape(slots, width).astype(BF16)
     gate_part = dot32(rows_in, eg[0])
     up_part = dot32(rows_in, eu[0])
     activation = (jax.nn.silu(gate_part) * up_part).astype(BF16)
 
-    def send_back(i, c, from_core):
+    def send_back(i, c):
         there = peer(i)
         return pltpu.make_async_remote_copy(
-            src_ref=results.at[c, there],
+            src_ref=results.at[c * n_ep + there],
             dst_ref=returned.at[me * n_tp + core],
-            send_sem=back_send.at[c, i],
-            recv_sem=back_recv.at[from_core, i],
+            send_sem=back_send,
+            recv_sem=back_recv,
             device_id=(there, c),
             device_id_type=MESH,
         )
 
     for c in range(n_tp):
         result = dot32(activation, ed[0, :, c * half : (c + 1) * half])
-        results[c] = result.reshape(n_ep, cap, half).astype(BF16)
-        over_peers(lambda i: send_back(i, c, core).start())
-    beside = pltpu.make_async_remote_copy(
-        src_ref=results.at[1 - core, me],
+        results[c * n_ep : (c + 1) * n_ep] = result.reshape(n_ep, cap, half).astype(BF16)
+        over_peers(lambda i: send_back(i, c).start())
+    pltpu.make_async_remote_copy(
+        src_ref=results.at[(1 - core) * n_ep + me],
         dst_ref=returned.at[me * n_tp + core],
-        send_sem=back_send.at[0, 0],
-        recv_sem=back_recv.at[0, 0],
+        send_sem=back_send,
+        recv_sem=back_recv,
         device_id=(me, 1 - core),
         device_id_type=MESH,
-    )
-    beside.start()
-    returned[me * n_tp + core] = results[core, me]
-
-    def home(i):
-        for c in range(n_tp):
-            send_back(i, c, c).wait()
-
-    over_peers(home)
-    beside.wait()
+    ).start()
+    returned[me * n_tp + core] = results[core * n_ep + me]
+    others = pl.ds(0, n_ep * n_tp - 1)
+    pltpu.make_async_remote_copy(
+        src_ref=results.at[others],
+        dst_ref=returned.at[others],
+        send_sem=back_send,
+        recv_sem=back_recv,
+        device_id=(me, 1 - core),
+        device_id_type=MESH,
+    ).wait()
     fetched = returned[...].astype(F32).reshape(slots * n_tp, half).astype(BF16)
     down = (((0,), (0,)), ((), ()))
     blended = (
@@ -352,15 +390,13 @@
     ).astype(BF16)
 
 
-def store_kernel(chunk, out_ref, fresh, out_hbm, new_hbm, out_sem, new_sem):
-    copies = [pltpu.make_async_copy(out_ref, out_hbm, out_sem)]
-    for n in range(fresh.shape[0] // chunk):
-        part = pl.ds(n * chunk, chunk)
-        copies.append(pltpu.make_async_copy(fresh.at[part], new_hbm.at[part], new_sem.at[n]))
-    for one in copies:
-        one.start()
-    for one in copies:
-        one.wait()
+def store_kernel(out_ref, fresh, out_hbm, new_hbm, out_sem, new_sem):
+    for part in pieces(fresh.shape, fresh.dtype):
+        pltpu.make_async_copy(fresh.at[part], new_hbm.at[part], new_sem).start()
+    last = pltpu.make_async_copy(out_ref, out_hbm, out_sem)
+    last.start()
+    last.wait()
+    pltpu.make_async_copy(fresh, new_hbm, new_sem).wait()
 
 
 def on_device(
@@ -435,7 +471,7 @@
             pltpu.VMEM((rows, width), BF16),
             pltpu.VMEM((n_ep, cap, width), BF16),
             pltpu.VMEM((n_ep, cap, width), BF16),
-            pltpu.VMEM((n_tp, n_ep, cap, half), BF16),
+            pltpu.VMEM((n_tp * n_ep, cap, half), BF16),
             pltpu.VMEM((n_ep * n_tp, cap, half), BF16),
             pltpu.VMEM((rows, 128), F32),
             pltpu.VMEM((rows, 128), F32),
@@ -443,10 +479,10 @@
             dma((chunks,)),
             dma((2,)),
             dma((2,)),
-            dma((n_ep,)),
-            dma((n_ep,)),
-            dma((n_tp, n_ep)),
-            dma((n_tp, n_ep)),
+            dma,
+            dma,
+            dma,
+            dma,
         ],
         compiler_params=pltpu.CompilerParams(
             collective_id=0, has_side_effects=True, vmem_limit_bytes=40 * 1024 * 1024
@@ -454,14 +490,14 @@
         name="layer",
     )(*pinned(operands))
     return pl.pallas_call(
-        functools.partial(store_kernel, chunk),
+        store_kernel,
         out_shape=(
             jax.ShapeDtypeStruct(new_tokens.shape, BF16),
             jax.ShapeDtypeStruct(new_state.shape, F32),
         ),
         in_specs=[vmem, vmem],
         out_specs=(in_hbm, in_hbm),
-        scratch_shapes=[dma, dma((chunks,))],
+        scratch_shapes=[dma, dma],
         compiler_params=pltpu.CompilerParams(vmem_limit_bytes=8 * 1024 * 1024),
         name="store",
     )(new_tokens, new_state)

time: 28 us -> 25.8 us (0.921)
  Pallas kernels: 27.2 us -> 25 us
    pallas_call x1, Pallas kernels: 25.1 us -> 23 us  [on_device(): pl.pallas_call(functools.partial(layer_kernel, n_ep, n_tp, cap, chunk), o...]
where the time goes in v2:
time: 25.8 us; the launch traced here: 25.6 us
  Pallas kernels  25 us (97%)
  between operations  0.65 us (3%)
    pallas_call x1, Pallas kernels, on_device(): pl.pallas_call(functools.partial(layer_kernel, n_ep, n_tp, cap, chunk), o...  23 us
    pallas_call x1, Pallas kernels, on_device(): pl.pallas_call(store_kernel, out_shape=(jax.ShapeDtypeStruct(new_tokens.s...  2.01 us

profile of v2, /device:TPU:0, one launch (start us, length us, event | category | flops | bytes accessed | tf_op | source)
XLA Modules:
  0.0 25.6 jit_solution(12805898599926446710)
XLA Ops:
  0.6 23.0 %layer.1 = (bf16[16,1024]{1,0:T(8,128)(2,1)S(1)}, f32[16,2,128,256]{3,2,1,0:T(8,128)S(1)}) custom-call(bf16[16,2048]{1,0:T(8,128)(2,1)} %tokens_hbm.1, f32[16,2,128,256]{3,2,1,0:T(8,128)} %state_hbm.1, bf16[2048,256]{1,0:T(8,128)(2,1)} %wq_hbm.1, bf16[2048,256]{1,0:T(8,128)(2,1)} %wk_hbm.1, bf16[2048,256]{1,0:T(8,128)(2,1)} %wd_hbm.1, ...), custom_call_target="tpu_custom_call" | custom-call | tf_op jit(solution)/shard_map/layer/pallas_call | solution.py:459
  23.6 2.0 %store.1 = (bf16[16,1024]{1,0:T(8,128)(2,1)}, f32[16,2,128,256]{3,2,1,0:T(8,128)}) custom-call(bf16[16,1024]{1,0:T(8,128)(2,1)S(1)} %get-tuple-element.4.out_ref, f32[16,2,128,256]{3,2,1,0:T(8,128)S(1)} %get-tuple-element.5.fresh), custom_call_target="tpu_custom_call" | custom-call | tf_op jit(solution)/shard_map/store/pallas_call | solution.py:492

commit v3 on v2

--- a/solution.py
+++ b/solution.py
@@ -98,10 +98,11 @@
     per_group = router_w.shape[0] // group_w.shape[0]
     slots = n_ep * cap
     chunks = rows // chunk
-    unrolled = n_ep <= 32
+
+    unrolled = n_ep <= 32 and n_ep & (n_ep - 1) == 0
 
     def peer(i):
-        if not unrolled or n_ep & (n_ep - 1):
+        if not unrolled:
             return lax.rem(me + i, n_ep)
         there = me
         bit = 1
@@ -124,6 +125,9 @@
                 return carry
 
             lax.fori_loop(1, n_ep, step, 0)
+
+    batches = ((0, 1), (1, n_ep // 2 - 1), (n_ep // 2, n_ep // 2))
+    own_batch = lax.div(me + n_ep - 1, n_ep) + lax.div(me, n_ep // 2)
 
     names = (
         ("routes", routes_hbm, routes),
@@ -275,20 +279,11 @@
             src_ref=outgoing.at[there],
             dst_ref=arrived.at[me],
             send_sem=go_send,
-            recv_sem=go_recv,
+            recv_sem=go_recv.at[own_batch],
             device_id=(there, core),
             device_id_type=MESH,
         )
 
-    others = pl.ds(0, n_ep - 1)
-    all_out = pltpu.make_async_remote_copy(
-        src_ref=outgoing.at[others],
-        dst_ref=arrived.at[others],
-        send_sem=go_send,
-        recv_sem=go_recv,
-        device_id=(peer(1), core),
-        device_id_type=MESH,
-    )
     over_peers(lambda i: dispatch(i).start())
     arrived[me] = outgoing[me]
 
@@ -321,14 +316,7 @@
     for name in ("eg", "eu", "ed"):
         ready(name)
 
-    all_out.wait()
-    rows_in = arrived[...].astype(F32).reshape(slots, width).astype(BF16)
-    gate_part = dot32(rows_in, eg[0])
-    up_part = dot32(rows_in, eu[0])
-    activation = (jax.nn.silu(gate_part) * up_part).astype(BF16)
-
-    def send_back(i, c):
-        there = peer(i)
+    def send_back(there, c):
         return pltpu.make_async_remote_copy(
             src_ref=results.at[c * n_ep + there],
             dst_ref=returned.at[me * n_tp + core],
@@ -338,10 +326,37 @@
             device_id_type=MESH,
         )
 
-    for c in range(n_tp):
-        result = dot32(activation, ed[0, :, c * half : (c + 1) * half])
-        results[c * n_ep : (c + 1) * n_ep] = result.reshape(n_ep, cap, half).astype(BF16)
-        over_peers(lambda i: send_back(i, c).start())
+    def landed(batch, count):
+        some = arrived.at[pl.ds(0, count)]
+        pltpu.make_async_copy(some, some, go_recv.at[batch]).wait()
+
+    def serve(batch):
+        start, size = batches[batch]
+        if size > 1:
+            pl.when(own_batch == batch)(lambda: landed(batch, size - 1))
+        pl.when(own_batch != batch)(lambda: landed(batch, size))
+        rows_in = arrived[start : start + size].astype(F32)
+        rows_in = rows_in.reshape(size * cap, width).astype(BF16)
+        gate_part = dot32(rows_in, eg[0])
+        up_part = dot32(rows_in, eu[0])
+        activation = (jax.nn.silu(gate_part) * up_part).astype(BF16)
+        for c in range(n_tp):
+            at = c * n_ep + start
+            result = dot32(activation, ed[0, :, c * half : (c + 1) * half])
+            results[at : at + size] = result.reshape(size, cap, half).astype(BF16)
+            if size == 1:
+                pl.when(own_batch != batch)(lambda: send_back(start, c).start())
+                continue
+
+            def back(i):
+                there = peer(i)
+                pl.when((there >= start) & (there < start + size))(lambda: send_back(there, c).start())
+
+            over_peers(back)
+
+    serve(0)
+    serve(1)
+    serve(2)
     pltpu.make_async_remote_copy(
         src_ref=results.at[(1 - core) * n_ep + me],
         dst_ref=returned.at[me * n_tp + core],
@@ -351,15 +366,11 @@
         device_id_type=MESH,
     ).start()
     returned[me * n_tp + core] = results[core * n_ep + me]
+    others = pl.ds(0, n_ep - 1)
+    pltpu.make_async_copy(outgoing.at[others], outgoing.at[others], go_send).wait()
     others = pl.ds(0, n_ep * n_tp - 1)
-    pltpu.make_async_remote_copy(
-        src_ref=results.at[others],
-        dst_ref=returned.at[others],
-        send_sem=back_send,
-        recv_sem=back_recv,
-        device_id=(me, 1 - core),
-        device_id_type=MESH,
-    ).wait()
+    pltpu.make_async_copy(returned.at[others], returned.at[others], back_recv).wait()
+    pltpu.make_async_copy(results.at[others], results.at[others], back_send).wait()
     fetched = returned[...].astype(F32).reshape(slots * n_tp, half).astype(BF16)
     down = (((0,), (0,)), ((), ()))
     blended = (
@@ -480,7 +491,7 @@
             dma((2,)),
             dma((2,)),
             dma,
-            dma,
+            dma((3,)),
             dma,
             dma,
         ],

time: 25.8 us -> 23.7 us (0.919)
  the two profiles are of different devices: /device:TPU:0 before, /device:TPU:5 now
where the time goes in v3:
time: 23.7 us; the launch traced here: 23.5 us
  Pallas kernels  22.8 us (96%)
  between operations  0.65 us (3%)
    pallas_call x1, Pallas kernels, on_device(): pl.pallas_call(functools.partial(layer_kernel, n_ep, n_tp, cap, chunk), o...  20.8 us
    pallas_call x1, Pallas kernels, on_device(): pl.pallas_call(store_kernel, out_shape=(jax.ShapeDtypeStruct(new_tokens.s...  2.01 us

profile of v3, /device:TPU:5, one launch (start us, length us, event | category | flops | bytes accessed | tf_op | source)
XLA Modules:
  0.0 23.5 jit_solution(6565343434919381351)
XLA Ops:
  0.6 20.8 %layer.1 = (bf16[16,1024]{1,0:T(8,128)(2,1)S(1)}, f32[16,2,128,256]{3,2,1,0:T(8,128)S(1)}) custom-call(bf16[16,2048]{1,0:T(8,128)(2,1)} %tokens_hbm.1, f32[16,2,128,256]{3,2,1,0:T(8,128)} %state_hbm.1, bf16[2048,256]{1,0:T(8,128)(2,1)} %wq_hbm.1, bf16[2048,256]{1,0:T(8,128)(2,1)} %wk_hbm.1, bf16[2048,256]{1,0:T(8,128)(2,1)} %wd_hbm.1, ...), custom_call_target="tpu_custom_call" | custom-call | tf_op jit(solution)/shard_map/layer/pallas_call | solution.py:470
  21.5 2.0 %store.1 = (bf16[16,1024]{1,0:T(8,128)(2,1)}, f32[16,2,128,256]{3,2,1,0:T(8,128)}) custom-call(bf16[16,1024]{1,0:T(8,128)(2,1)S(1)} %get-tuple-element.4.out_ref, f32[16,2,128,256]{3,2,1,0:T(8,128)S(1)} %get-tuple-element.5.fresh), custom_call_target="tpu_custom_call" | custom-call | tf_op jit(solution)/shard_map/store/pallas_call | solution.py:503

commit v4 on v3

--- a/solution.py
+++ b/solution.py
@@ -13,8 +13,8 @@
 eps_norm = 1e-05
 F32 = jnp.float32
 BF16 = jnp.bfloat16
-PIECE = 128 * 1024
-AHEAD = 8 * 1024 * 1024
+PIECE = 256 * 1024
+AHEAD = 7 * 1024 * 1024
 
 
 def dot32(a, b):
@@ -101,10 +101,18 @@
 
     unrolled = n_ep <= 32 and n_ep & (n_ep - 1) == 0
 
+    own_side = lax.div(me, n_ep // 2)
+
     def peer(i):
         if not unrolled:
             return lax.rem(me + i, n_ep)
-        there = me
+        planes = n_ep // 4
+        if i >= n_ep // 2 and planes > 1:
+            plane = i // 4 + own_side * (planes - 1 - 2 * (i // 4))
+            there = plane * 4 + lax.rem(me, 4)
+            i = i % 4
+        else:
+            there = me
         bit = 1
         while bit < n_ep:
             if i & bit:
@@ -126,8 +134,8 @@
 
             lax.fori_loop(1, n_ep, step, 0)
 
-    batches = ((0, 1), (1, n_ep // 2 - 1), (n_ep // 2, n_ep // 2))
-    own_batch = lax.div(me + n_ep - 1, n_ep) + lax.div(me, n_ep // 2)
+    batches = ((0, 1), (1, n_ep // 4 - 1), (n_ep // 4, n_ep // 4), (n_ep // 2, n_ep // 2))
+    own_batch = lax.div(me + n_ep - 1, n_ep) + lax.div(me, n_ep // 4) - lax.div(me, 3 * (n_ep // 4))
 
     names = (
         ("routes", routes_hbm, routes),
@@ -248,7 +256,10 @@
         scale = lax.rsqrt(jnp.mean(r * r, axis=-1, keepdims=True) + eps_norm)
         gated.append((r * scale * head_gain[...] * jax.nn.silu(gate[:, part])).astype(BF16))
     ready("wo")
-    part_mine[...] = dot32(jnp.concatenate(gated, axis=1), wo[...]).astype(BF16)
+    gated = jnp.concatenate(gated, axis=1)
+    for c in range(n_tp):
+        part = slice(c * half, (c + 1) * half)
+        part_mine[:, part] = dot32(gated, wo[:, part]).astype(BF16)
 
     pl.semaphore_wait(barrier, n_ep * n_tp - 1)
     swap = pltpu.make_async_remote_copy(
@@ -287,12 +298,14 @@
     over_peers(lambda i: dispatch(i).start())
     arrived[me] = outgoing[me]
 
-    columns = as_columns([keys, decay])
-    for b in range(rows):
-        for h in range(heads):
-            col = columns[h]
-            v = values[b : b + 1, h * value_dim : (h + 1) * value_dim]
-            fresh[b, h] = col[:, rows + b : rows + b + 1] * state[b, h] + col[:, b : b + 1] * v
+    @pl.when(me >= 0)
+    def _():
+        columns = as_columns([keys, decay])
+        for b in range(rows):
+            for h in range(heads):
+                col = columns[h]
+                v = values[b : b + 1, h * value_dim : (h + 1) * value_dim]
+                fresh[b, h] = col[:, rows + b : rows + b + 1] * state[b, h] + col[:, b : b + 1] * v
 
     across = (((1,), (1,)), ((), ()))
     group_logit = lax.dot_general(group_w[...], hidden, across, preferred_element_type=F32)
@@ -357,6 +370,7 @@
     serve(0)
     serve(1)
     serve(2)
+    serve(3)
     pltpu.make_async_remote_copy(
         src_ref=results.at[(1 - core) * n_ep + me],
         dst_ref=returned.at[me * n_tp + core],
@@ -491,7 +505,7 @@
             dma((2,)),
             dma((2,)),
             dma,
-            dma((3,)),
+            dma((4,)),
             dma,
             dma,
         ],

time: 23.7 us -> 23.2 us (0.979)
  the two profiles are of different devices: /device:TPU:5 before, /device:TPU:17 now
where the time goes in v4:
time: 23.2 us; the launch traced here: 23 us
  Pallas kernels  22.4 us (97%)
  between operations  0.65 us (3%)
    pallas_call x1, Pallas kernels, on_device(): pl.pallas_call(functools.partial(layer_kernel, n_ep, n_tp, cap, chunk), o...  20.4 us
    pallas_call x1, Pallas kernels, on_device(): pl.pallas_call(store_kernel, out_shape=(jax.ShapeDtypeStruct(new_tokens.s...  2.01 us

profile of v4, /device:TPU:17, one launch (start us, length us, event | category | flops | bytes accessed | tf_op | source)
XLA Modules:
  0.0 23.0 jit_solution(8106748364325726676)
XLA Ops:
  0.6 20.4 %layer.1 = (bf16[16,1024]{1,0:T(8,128)(2,1)S(1)}, f32[16,2,128,256]{3,2,1,0:T(8,128)S(1)}) custom-call(bf16[16,2048]{1,0:T(8,128)(2,1)} %tokens_hbm.1, f32[16,2,128,256]{3,2,1,0:T(8,128)} %state_hbm.1, bf16[2048,256]{1,0:T(8,128)(2,1)} %wq_hbm.1, bf16[2048,256]{1,0:T(8,128)(2,1)} %wk_hbm.1, bf16[2048,256]{1,0:T(8,128)(2,1)} %wd_hbm.1, ...), custom_call_target="tpu_custom_call" | custom-call | tf_op jit(solution)/shard_map/layer/pallas_call | solution.py:484
  21.0 2.0 %store.1 = (bf16[16,1024]{1,0:T(8,128)(2,1)}, f32[16,2,128,256]{3,2,1,0:T(8,128)}) custom-call(bf16[16,1024]{1,0:T(8,128)(2,1)S(1)} %get-tuple-element.4.out_ref, f32[16,2,128,256]{3,2,1,0:T(8,128)S(1)} %get-tuple-element.5.fresh), custom_call_target="tpu_custom_call" | custom-call | tf_op jit(solution)/shard_map/store/pallas_call | solution.py:517

commit v5 on v4

--- a/solution.py
+++ b/solution.py
@@ -14,7 +14,7 @@
 F32 = jnp.float32
 BF16 = jnp.bfloat16
 PIECE = 256 * 1024
-AHEAD = 7 * 1024 * 1024
+AHEAD = 11 * 1024 * 1024
 
 
 def dot32(a, b):
@@ -82,6 +82,7 @@
     stat_mine,
     stat_other,
     in_sem,
+    wo_sem,
     state_sem,
     pair_sem,
     stat_sem,
@@ -146,7 +147,6 @@
         ("wv", wv_hbm, wv),
         ("wg", wg_hbm, wg),
         ("head_gain", gain_hbm, head_gain),
-        ("wo", wo_hbm, wo),
         ("norm_gain", norm_gain_hbm, norm_gain),
         ("norm_bias", norm_bias_hbm, norm_bias),
         ("group_w", group_w_hbm, group_w),
@@ -156,14 +156,19 @@
         ("ed", ed_hbm, ed),
     )
     load = {name: (src, dst, in_sem.at[n]) for n, (name, src, dst) in enumerate(names)}
+    for c in range(n_tp):
+        part = (slice(None), pl.ds(c * half, half))
+        load["wo", c] = (wo_hbm.at[part], wo.at[part], wo_sem.at[c])
     for n in range(chunks):
         part = pl.ds(n * chunk, chunk)
         load[n] = (state_hbm.at[part], state.at[part], state_sem.at[n])
 
-    def fetch(name):
+    def fetch(name, urgent):
         src, dst, sem = load[name]
         for part in pieces(src.shape, src.dtype):
-            pltpu.make_async_copy(src.at[part], dst.at[part], sem).start()
+            pltpu.make_async_copy(src.at[part], dst.at[part], sem).start(
+                priority=0 if urgent else 1
+            )
 
     def ready(name):
         pltpu.make_async_copy(*load[name]).wait()
@@ -171,7 +176,8 @@
         fetch_more()
 
     queue = [*("routes", "tokens", "wd", "wq"), *range(chunks), *("wk", "wv", "head_gain", "wg")]
-    queue += ["wo", "norm_gain", "norm_bias", "group_w", "router_w", "eg", "eu", "ed"]
+    queue += [*(("wo", c) for c in range(n_tp)), "norm_gain", "norm_bias", "group_w", "router_w", "eg", "eu", "ed"]
+    urgent = queue[: 4 + chunks]
     flying = {}
 
     def fetch_more():
@@ -179,7 +185,7 @@
             name = queue.pop(0)
             src = load[name][0]
             flying[name] = math.prod(src.shape) * jnp.dtype(src.dtype).itemsize
-            fetch(name)
+            fetch(name, name in urgent)
 
     fetch_more()
 
@@ -255,9 +261,9 @@
         r = readout[:, part] + meet * values[:, part]
         scale = lax.rsqrt(jnp.mean(r * r, axis=-1, keepdims=True) + eps_norm)
         gated.append((r * scale * head_gain[...] * jax.nn.silu(gate[:, part])).astype(BF16))
-    ready("wo")
     gated = jnp.concatenate(gated, axis=1)
     for c in range(n_tp):
+        ready(("wo", c))
         part = slice(c * half, (c + 1) * half)
         part_mine[:, part] = dot32(gated, wo[:, part]).astype(BF16)
 
@@ -500,7 +506,8 @@
             pltpu.VMEM((n_ep * n_tp, cap, half), BF16),
             pltpu.VMEM((rows, 128), F32),
             pltpu.VMEM((rows, 128), F32),
-            dma((len(operands) - 1,)),
+            dma((len(operands) - 2,)),
+            dma((n_tp,)),
             dma((chunks,)),
             dma((2,)),
             dma((2,)),

time: 23.2 us -> 23 us (level)
  no operation moved by 1% of the time
where the time goes in v5:
time: 23 us; the launch traced here: 22.9 us
  Pallas kernels  22.2 us (97%)
  between operations  0.65 us (3%)
    pallas_call x1, Pallas kernels, on_device(): pl.pallas_call(functools.partial(layer_kernel, n_ep, n_tp, cap, chunk), o...  20.2 us
    pallas_call x1, Pallas kernels, on_device(): pl.pallas_call(store_kernel, out_shape=(jax.ShapeDtypeStruct(new_tokens.s...  2.01 us

profile of v5, /device:TPU:17, one launch (start us, length us, event | category | flops | bytes accessed | tf_op | source)
XLA Modules:
  0.0 22.9 jit_solution(12835491679507243644)
XLA Ops:
  0.6 20.2 %layer.1 = (bf16[16,1024]{1,0:T(8,128)(2,1)S(1)}, f32[16,2,128,256]{3,2,1,0:T(8,128)S(1)}) custom-call(bf16[16,2048]{1,0:T(8,128)(2,1)} %tokens_hbm.1, f32[16,2,128,256]{3,2,1,0:T(8,128)} %state_hbm.1, bf16[2048,256]{1,0:T(8,128)(2,1)} %wq_hbm.1, bf16[2048,256]{1,0:T(8,128)(2,1)} %wk_hbm.1, bf16[2048,256]{1,0:T(8,128)(2,1)} %wd_hbm.1, ...), custom_call_target="tpu_custom_call" | custom-call | tf_op jit(solution)/shard_map/layer/pallas_call | solution.py:490
  20.8 2.0 %store.1 = (bf16[16,1024]{1,0:T(8,128)(2,1)}, f32[16,2,128,256]{3,2,1,0:T(8,128)}) custom-call(bf16[16,1024]{1,0:T(8,128)(2,1)S(1)} %get-tuple-element.4.out_ref, f32[16,2,128,256]{3,2,1,0:T(8,128)S(1)} %get-tuple-element.5.fresh), custom_call_target="tpu_custom_call" | custom-call | tf_op jit(solution)/shard_map/store/pallas_call | solution.py:524

commit v6 on v5

--- a/solution.py
+++ b/solution.py
@@ -54,6 +54,8 @@
     eu_hbm,
     ed_hbm,
     out_ref,
+    stat_ref,
+    scale_ref,
     fresh,
     tokens,
     state,
@@ -403,6 +405,9 @@
     lane = lax.broadcasted_iota(jnp.int32, stat_mine.shape, 1)
     stats = jnp.where(lane == 0, total, squares)
     stat_mine[...] = stats
+    out_ref[...] = blended
+    scale_ref[0:1, :] = gain
+    scale_ref[1:2, :] = shift
     trade = pltpu.make_async_remote_copy(
         src_ref=stat_mine,
         dst_ref=stat_other,
@@ -413,18 +418,18 @@
     )
     trade.start()
     trade.wait()
-    both = stats + stat_other[...]
-    row_mean = both[:, 0:1] / width
-    spread = both[:, 1:2] / width - row_mean * row_mean
-    out_ref[...] = (
-        (blended - row_mean) * lax.rsqrt(spread + eps_norm) * gain + shift
-    ).astype(BF16)
-
-
-def store_kernel(out_ref, fresh, out_hbm, new_hbm, out_sem, new_sem):
+    stat_ref[...] = stats + stat_other[...]
+
+
+def store_kernel(width, blended, stats, scale, fresh, out_hbm, new_hbm, out, out_sem, new_sem):
     for part in pieces(fresh.shape, fresh.dtype):
         pltpu.make_async_copy(fresh.at[part], new_hbm.at[part], new_sem).start()
-    last = pltpu.make_async_copy(out_ref, out_hbm, out_sem)
+    row_mean = stats[:, 0:1] / width
+    spread = stats[:, 1:2] / width - row_mean * row_mean
+    out[...] = (
+        (blended[...] - row_mean) * lax.rsqrt(spread + eps_norm) * scale[0:1, :] + scale[1:2, :]
+    ).astype(BF16)
+    last = pltpu.make_async_copy(out, out_hbm, out_sem)
     last.start()
     last.wait()
     pltpu.make_async_copy(fresh, new_hbm, new_sem).wait()
@@ -487,14 +492,16 @@
         expert_up,
         expert_down,
     )
-    new_tokens, new_state = pl.pallas_call(
+    blended, stats, scale, fresh = pl.pallas_call(
         functools.partial(layer_kernel, n_ep, n_tp, cap, chunk),
         out_shape=(
-            jax.ShapeDtypeStruct((rows, half), BF16),
+            jax.ShapeDtypeStruct((rows, half), F32),
+            jax.ShapeDtypeStruct((rows, 128), F32),
+            jax.ShapeDtypeStruct((2, half), F32),
             jax.ShapeDtypeStruct(recurrent_state.shape, F32),
         ),
         in_specs=[in_hbm] * len(operands),
-        out_specs=(vmem, vmem),
+        out_specs=(vmem,) * 4,
         scratch_shapes=[like(a) for a in operands]
         + [
             pltpu.VMEM((rows, heads * value_dim), F32),
@@ -522,17 +529,17 @@
         name="layer",
     )(*pinned(operands))
     return pl.pallas_call(
-        store_kernel,
+        functools.partial(store_kernel, width),
         out_shape=(
-            jax.ShapeDtypeStruct(new_tokens.shape, BF16),
-            jax.ShapeDtypeStruct(new_state.shape, F32),
+            jax.ShapeDtypeStruct((rows, half), BF16),
+            jax.ShapeDtypeStruct(fresh.shape, F32),
         ),
-        in_specs=[vmem, vmem],
+        in_specs=[vmem] * 4,
         out_specs=(in_hbm, in_hbm),
-        scratch_shapes=[dma, dma],
+        scratch_shapes=[pltpu.VMEM((rows, half), BF16), dma, dma],
         compiler_params=pltpu.CompilerParams(vmem_limit_bytes=8 * 1024 * 1024),
         name="store",
-    )(new_tokens, new_state)
+    )(blended, stats, scale, fresh)
 
 
 def solution(mesh):

time: 23 us -> 22.9 us (level)
  no operation moved by 1% of the time
where the time goes in v6:
time: 22.9 us; the launch traced here: 22.7 us
  Pallas kernels  22.1 us (97%)
  between operations  0.65 us (3%)
    pallas_call x1, Pallas kernels, on_device(): pl.pallas_call(functools.partial(layer_kernel, n_ep, n_tp, cap, chunk), o...  20 us
    pallas_call x1, Pallas kernels, on_device(): pl.pallas_call(functools.partial(store_kernel, width), out_shape=(jax.Sha...  2.01 us

profile of v6, /device:TPU:17, one launch (start us, length us, event | category | flops | bytes accessed | tf_op | source)
XLA Modules:
  0.0 22.7 jit_solution(4320017208157636794)
XLA Ops:
  0.6 20.0 %layer.1 = (f32[16,1024]{1,0:T(8,128)S(1)}, f32[16,128]{1,0:T(8,128)S(1)}, f32[2,1024]{1,0:T(2,128)S(1)}, f32[16,2,128,256]{3,2,1,0:T(8,128)S(1)}) custom-call(bf16[16,2048]{1,0:T(8,128)(2,1)} %tokens_hbm.1, f32[16,2,128,256]{3,2,1,0:T(8,128)} %state_hbm.1, bf16[2048,256]{1,0:T(8,128)(2,1)} %wq_hbm.1, bf16[2048,256]{1,0:T(8,128)(2,1)} %wk_hbm.1, ...), custom_call_target="tpu_custom_call" | custom-call | tf_op jit(solution)/shard_map/layer/pallas_call | solution.py:495
  20.7 2.0 %store.1 = (bf16[16,1024]{1,0:T(8,128)(2,1)}, f32[16,2,128,256]{3,2,1,0:T(8,128)}) custom-call(f32[16,1024]{1,0:T(8,128)S(1)} %get-tuple-element.6.blended, f32[16,128]{1,0:T(8,128)S(1)} %get-tuple-element.7.stats, f32[2,1024]{1,0:T(2,128)S(1)} %get-tuple-element.8.scale, f32[16,2,128,256]{3,2,1,0:T(8,128)S(1)} %get-tuple-element.9.fresh), custom_call_target="tpu_custom_call" | custom-call | tf_op jit(solution)/shard_map/store/pallas_call | solution.py:531

commit v7 on v6

--- a/solution.py
+++ b/solution.py
@@ -460,7 +460,7 @@
     heads, key_dim, value_dim = recurrent_state.shape[1:]
     in_hbm = pl.BlockSpec(memory_space=pltpu.HBM)
     vmem = pl.BlockSpec(memory_space=pltpu.VMEM)
-    chunk = 4
+    chunk = 8
     chunks = rows // chunk
     dma = pltpu.SemaphoreType.DMA
 

time: 22.9 us -> 22.9 us (level)
  no operation moved by 1% of the time
where the time goes in v7:
time: 22.9 us; the launch traced here: 22.7 us
  Pallas kernels  22 us (96%)
  between operations  0.65 us (3%)
    pallas_call x1, Pallas kernels, on_device(): pl.pallas_call(functools.partial(layer_kernel, n_ep, n_tp, cap, chunk), o...  20 us
    pallas_call x1, Pallas kernels, on_device(): pl.pallas_call(functools.partial(store_kernel, width), out_shape=(jax.Sha...  2.01 us

profile of v7, /device:TPU:17, one launch (start us, length us, event | category | flops | bytes accessed | tf_op | source)
XLA Modules:
  0.0 22.7 jit_solution(10447408774999119238)
XLA Ops:
  0.6 20.0 %layer.1 = (f32[16,1024]{1,0:T(8,128)S(1)}, f32[16,128]{1,0:T(8,128)S(1)}, f32[2,1024]{1,0:T(2,128)S(1)}, f32[16,2,128,256]{3,2,1,0:T(8,128)S(1)}) custom-call(bf16[16,2048]{1,0:T(8,128)(2,1)} %tokens_hbm.1, f32[16,2,128,256]{3,2,1,0:T(8,128)} %state_hbm.1, bf16[2048,256]{1,0:T(8,128)(2,1)} %wq_hbm.1, bf16[2048,256]{1,0:T(8,128)(2,1)} %wk_hbm.1, ...), custom_call_target="tpu_custom_call" | custom-call | tf_op jit(solution)/shard_map/layer/pallas_call | solution.py:495
  20.7 2.0 %store.1 = (bf16[16,1024]{1,0:T(8,128)(2,1)}, f32[16,2,128,256]{3,2,1,0:T(8,128)}) custom-call(f32[16,1024]{1,0:T(8,128)S(1)} %get-tuple-element.6.blended, f32[16,128]{1,0:T(8,128)S(1)} %get-tuple-element.7.stats, f32[2,1024]{1,0:T(2,128)S(1)} %get-tuple-element.8.scale, f32[16,2,128,256]{3,2,1,0:T(8,128)S(1)} %get-tuple-element.9.fresh), custom_call_target="tpu_custom_call" | custom-call | tf_op jit(solution)/shard_map/store/pallas_call | solution.py:531
